TPU v7x, 32 devices: a whole 2x2x4 slice. The times are simulated.
32 devices in a mesh: ep: 4 (over y, x), tp: 8 (over z, core).
Axes of the slice: x: 2, y: 2, z: 4, core: 2. Of those that a mesh axis runs over, the one named last changes fastest.
Arguments:
- query_heads_rows: bfloat16 [2048, 2048], P('ep', 'tp'), may hold values from -9 to 9
- key_heads_rows: bfloat16 [2048, 2048], P('ep', 'tp'), may hold values from -9 to 9
- value_heads_rows: bfloat16 [2048, 2048], P('ep', 'tp'), may hold values from -6 to 6
- write_strength_logit: bfloat16 [16, 2048], P('tp', 'ep'), may hold values from -3.5 to -1
- decay_preactivation: bfloat16 [16, 2048], P('tp', 'ep'), may hold values from -5 to 5
- head_decay_logarithm: float32 [16], P('tp'), may hold values from -20 to -3
- extra_log_decay: float32 [16, 2048], P('tp', 'ep'), may hold values from -0.7 to 0
- output_weight: bfloat16 [2048, 2048], P('tp'), may hold values from -2 to 2
- second_batch_tokens: bfloat16 [4096, 2048], P(('ep', 'tp')), may hold values from -6 to 6
- expert_norm_scale: float32 [2048], replicated, may hold values from 0.1 to 1.9
- expert_choice_index: int32 [4096, 2], P(('ep', 'tp')), may hold values from 0 to 15, as said below
- group_router_weight: float32 [4096], P(('ep', 'tp')), may hold values from 0.25 to 1
- expert_logit_difference: float32 [4096], P(('ep', 'tp')), may hold values from -8 to 8
- expert_gate_weight: bfloat16 [16, 1024, 2048], P('ep', 'tp'), may hold values from -0.125 to 0.125
- expert_up_weight: bfloat16 [16, 1024, 2048], P('ep', 'tp'), may hold values from -0.125 to 0.125
- expert_down_weight: bfloat16 [16, 1024, 2048], P('ep', 'tp'), may hold values from -0.375 to 0.375
Outputs:
- mixer_output_first: bfloat16 [2048, 2048], P(('ep', 'tp'))
- expert_out: bfloat16 [4096, 2048], P(('ep', 'tp'))
Inputs may be any that keep to these rules, and one draw needn't show every extreme that they name: `expert_choice_index`: each row names two different experts of one group, the experts a * 4 to a * 4 + 3 for some a. In the rows of one device (aligned blocks of 128 rows) no expert is named more than 32 times, and in every device's rows some expert is named exactly 32 times.
All inputs are finite; a program needn't handle non-finite values.
Results may differ from a plain program's by a relative error of at most 0.018.
Values may be sent and summed in bfloat16 or wider, within the bound.
A program may use at most 128 MiB of HBM per device.

v0:
```python
import jax
import jax.numpy as jnp
from jax import lax
from jax.sharding import PartitionSpec as P

DK = 128
DV = 128
BLOCK = 64
CAP = 32
EXPERTS = 16
TOPK = 2
precise_setting = lax.Precision.HIGHEST
norm_eps = 1e-06


def prefix(value, axis, join, neutral):
    count, mine = (lax.axis_size(axis), lax.axis_index(axis))
    pieces = jax.tree.map(lambda part: lax.all_gather(part, axis), value)
    subtotal = jax.tree.map(
        lambda part, zero: jnp.full_like(part, 0) + jnp.asarray(zero, part.dtype), value, neutral
    )

    def step(position, subtotal):
        longer = join(subtotal, jax.tree.map(lambda part: part[position], pieces))
        return jax.tree.map(lambda new, old: jnp.where(position < mine, new, old), longer, subtotal)

    return lax.fori_loop(0, count - 1, step, subtotal)


def unit_rows(matrix):
    return matrix * lax.rsqrt(jnp.sum(matrix * matrix, axis=-1, keepdims=True) + norm_eps)


def block_terms(query_block, key_block, value_block, decay_logarithm, strength):
    span_len = query_block.shape[2]
    dim_value = value_block.shape[-1]
    cumulative = jnp.cumsum(decay_logarithm, axis=-1)
    within = jnp.tril(jnp.ones((span_len, span_len), bool))
    strict = jnp.tril(jnp.ones((span_len, span_len), bool), -1)
    spread = cumulative[..., :, None] - cumulative[..., None, :]
    decayed = jnp.where(within, jnp.exp(jnp.where(within, spread, 0.0)), 0.0)
    weighted = key_block * strength[..., None]
    lower_part = jnp.where(
        strict,
        jnp.einsum("hnid,hnjd->hnij", weighted, key_block, precision=precise_setting) * decayed,
        0.0,
    )
    system = lower_part + jnp.eye(span_len, dtype=jnp.float32)
    rhs_cols = jnp.concatenate(
        [value_block * strength[..., None], weighted * jnp.exp(cumulative)[..., None]], axis=-1
    )
    solved = jax.scipy.linalg.solve_triangular(system, rhs_cols, lower=True, unit_diagonal=True)
    updated_values = solved[..., :dim_value]
    delta_corrections = solved[..., dim_value:]
    scores = jnp.where(
        within,
        jnp.einsum("hnid,hnjd->hnij", query_block, key_block, precision=precise_setting) * decayed,
        0.0,
    )
    decayed_queries = query_block * jnp.exp(cumulative)[..., None]
    decayed_keys = key_block * jnp.exp(cumulative[..., -1:] - cumulative)[..., None]
    block_retention = jnp.exp(cumulative[..., -1])
    return (
        decayed_queries,
        decayed_keys,
        updated_values,
        delta_corrections,
        scores,
        block_retention,
    )


def carry_step(recurrent_state, inputs):
    decayed_queries, decayed_keys, updated_values, delta_corrections, scores, block_retention = (
        inputs
    )
    value_updates = updated_values - jnp.einsum(
        "jdb,jbu->jdu", delta_corrections, recurrent_state, precision=precise_setting
    )
    final_output = jnp.einsum(
        "jdb,jbu->jdu", decayed_queries, recurrent_state, precision=precise_setting
    )
    final_output = final_output + jnp.einsum(
        "hcj,hjv->hcv", scores, value_updates, precision=precise_setting
    )
    recurrent_state = recurrent_state * block_retention[:, None, None] + jnp.einsum(
        "rpq,rpd->rqd", decayed_keys, value_updates, precision=precise_setting
    )
    return (recurrent_state, final_output)


def compose(earlier, latter):
    joined_map = jnp.einsum("hij,hjk->hik", latter[0], earlier[0], precision=precise_setting)
    joined_state = (
        jnp.einsum("hij,hjv->hiv", latter[0], earlier[1], precision=precise_setting) + latter[1]
    )
    return (joined_map, joined_state)


def shards(
    query_heads_rows,
    key_heads_rows,
    value_heads_rows,
    write_strength_logit,
    decay_preactivation,
    head_decay_logarithm,
    extra_log_decay,
    output_weight,
    second_batch_tokens,
    expert_norm_scale,
    expert_choice_index,
    group_router_weight,
    expert_logit_difference,
    expert_gate_weight,
    expert_up_weight,
    expert_down_weight,
):
    length = query_heads_rows.shape[0]
    local_heads = head_decay_logarithm.shape[0]
    blocks = length // BLOCK
    width_model = output_weight.shape[1]

    def heads_first(matrix):
        spread_out = matrix.astype(jnp.float32).reshape(length, local_heads, -1).transpose(1, 0, 2)
        return spread_out.reshape(local_heads, blocks, BLOCK, -1)

    query_block = unit_rows(heads_first(query_heads_rows)) * DK ** (-0.5)
    key_block = unit_rows(heads_first(key_heads_rows))
    value_block = heads_first(value_heads_rows)
    strength = jax.nn.sigmoid(write_strength_logit.astype(jnp.float32)).reshape(
        local_heads, blocks, BLOCK
    )
    decay_logarithm = (
        -jnp.exp(head_decay_logarithm)[:, None]
        * jax.nn.softplus(decay_preactivation.astype(jnp.float32))
        + extra_log_decay
    )
    decay_logarithm = decay_logarithm.reshape(local_heads, blocks, BLOCK)
    decayed_queries, decayed_keys, updated_values, delta_corrections, scores, block_retention = (
        block_terms(query_block, key_block, value_block, decay_logarithm, strength)
    )
    fresh_wide = jnp.concatenate(
        [updated_values, jnp.zeros(updated_values.shape[:-1] + (DK,), jnp.float32)], axis=-1
    )
    inputs = tuple(
        (
            jnp.moveaxis(term, 1, 0)
            for term in (
                decayed_queries,
                decayed_keys,
                fresh_wide,
                delta_corrections,
                scores,
                block_retention,
            )
        )
    )
    identity_map = jnp.broadcast_to(jnp.eye(DK, dtype=jnp.float32), (local_heads, DK, DK))
    start_memory = jnp.concatenate(
        [jnp.zeros((local_heads, DK, DV), jnp.float32), identity_map], axis=-1
    )
    end_memory, outputs = lax.scan(carry_step, start_memory, inputs)
    local_output = outputs[..., :DV]
    projection_matrix = outputs[..., DV:]
    carried_end = end_memory[..., :DV]
    transfer = end_memory[..., DV:]
    _, incoming_rows = prefix(
        (transfer, carried_end), "ep", compose, (identity_map, jnp.zeros_like(carried_end))
    )
    attention_result = local_output + jnp.einsum(
        "xtyg,tgd->xtyd", projection_matrix, incoming_rows, precision=precise_setting
    )
    attn_rows = (
        attention_result.transpose(0, 2, 1, 3)
        .reshape(length, local_heads * DV)
        .astype(jnp.bfloat16)
    )
    summed = lax.psum_scatter(
        jnp.dot(attn_rows, output_weight, preferred_element_type=jnp.float32).astype(jnp.bfloat16),
        "tp",
        scatter_dimension=0,
        tiled=True,
    )
    widened = second_batch_tokens.astype(jnp.float32)
    normed = (
        widened
        * lax.rsqrt(jnp.mean(widened * widened, axis=-1, keepdims=True) + norm_eps)
        * expert_norm_scale
    ).astype(jnp.bfloat16)
    own_tokens = second_batch_tokens.shape[0]
    ep_count = lax.axis_size("ep")
    local_experts = EXPERTS // ep_count
    flat_ids = expert_choice_index.reshape(-1)
    one_hot = (flat_ids[:, None] == jnp.arange(EXPERTS, dtype=jnp.int32)[None, :]).astype(jnp.int32)
    slot_rank = jnp.sum((jnp.cumsum(one_hot, axis=0) - one_hot) * one_hot, axis=1)
    slot_index = flat_ids * CAP + slot_rank
    copy_token = jnp.arange(flat_ids.shape[0], dtype=jnp.int32) // TOPK
    slot_token = jnp.full((EXPERTS * CAP,), own_tokens, jnp.int32).at[slot_index].set(copy_token)
    outgoing = jnp.take(normed, slot_token, axis=0, mode="fill", fill_value=0).reshape(
        ep_count, local_experts, CAP, width_model
    )
    arrived = lax.all_to_all(outgoing, "ep", split_axis=0, concat_axis=0, tiled=True)
    gate_piece = lax.all_gather(expert_gate_weight, "tp", axis=1, tiled=True)
    up_piece = lax.all_gather(expert_up_weight, "tp", axis=1, tiled=True)
    down_piece = lax.all_gather(expert_down_weight, "tp", axis=1, tiled=True)
    gating = jnp.einsum("secd,efd->secf", arrived, gate_piece, preferred_element_type=jnp.float32)
    upward = jnp.einsum("secd,efd->secf", arrived, up_piece, preferred_element_type=jnp.float32)
    hidden = (jax.nn.silu(gating) * upward).astype(jnp.bfloat16)
    produced = jnp.einsum("secf,efd->secd", hidden, down_piece, preferred_element_type=jnp.float32)
    returned = lax.all_to_all(
        produced.astype(jnp.bfloat16), "ep", split_axis=0, concat_axis=0, tiled=True
    )
    flat_results = returned.reshape(EXPERTS * CAP, width_model)
    picked = (
        jnp.take(flat_results, slot_index, axis=0)
        .reshape(own_tokens, TOPK, width_model)
        .astype(jnp.float32)
    )
    leading = jax.nn.sigmoid(expert_logit_difference)
    mixing = group_router_weight[:, None] * jnp.stack([leading, 1.0 - leading], axis=-1)
    expert_out = jnp.sum(mixing[..., None] * picked, axis=1).astype(jnp.bfloat16)
    return (summed, expert_out)


def solution(mesh):
    in_specs = (
        P("ep", "tp"),
        P("ep", "tp"),
        P("ep", "tp"),
        P("tp", "ep"),
        P("tp", "ep"),
        P("tp"),
        P("tp", "ep"),
        P("tp", None),
        P(("ep", "tp"), None),
        P(),
        P(("ep", "tp"), None),
        P(("ep", "tp")),
        P(("ep", "tp")),
        P("ep", "tp", None),
        P("ep", "tp", None),
        P("ep", "tp", None),
    )
    out_specs = (P(("ep", "tp"), None), P(("ep", "tp"), None))
    return jax.shard_map(shards, mesh=mesh, in_specs=in_specs, out_specs=out_specs, check_vma=False)
```

profile of v0, /device:TPU:0, one launch (start us, length us, event | category | flops | bytes accessed | tf_op | source)
XLA Modules:
  0.0 520.2 jit_solution(1640668718798541853)
XLA Ops:
  11.6 1.4 scatter_custom_fusion
  13.5 3.3 gather_fusion
  16.9 3.1 broadcast_select_fusion
  20.0 5.6 %all-to-all-start = ((bf16[4,4,32,2048]{3,2,1,0:T(8,128)(2,1)}), bf16[4,4,32,2048]{3,2,1,0:T(8,128)(2,1)S(1)}, u32[]{:S(2)}, u32[]{:S(2)}) async-start(bf16[4,4,32,2048]{3,2,1,0:T(8,128)(2,1)} %broadcast_select_fusion), calls=%async_computation.1 | async-start | bytes 4194304 | tf_op jit(solution)/shard_map/all_to_all | solution.py:202
  29.5 3.0 fusion.52
  32.4 80.0 %custom-call.4 = f32[2,8,1,64,64]{3,4,2,1,0:T(8,128)} custom-call(f32[2,8,1,64,64]{4,3,2,1,0:T(8,128)} %fusion.52), custom_call_target="InvertDiagBlocksLowerTriangular" | custom-call | tf_op jit(solution)/shard_map/jit(_solve_triangular)/vmap(vmap())/triangular_solve | solution.py:52
  114.4 2.0 copy.100
  119.9 2.5 multiply_multiply_fusion
  125.6 2.0 fusion.50
  128.6 48.9 %while.26 = (s32[]{:T(128)}, f32[2,128,256]{2,1,0:T(8,128)S(1)}, f32[8,2,64,256]{3,2,0,1:T(8,128)}, f32[8,2]{1,0:T(8,128)}, f32[8,2,64,128]{3,2,0,1:T(8,128)}, /...) while((s32[]{:T(128)}, f32[2,128,256]{2,1,0:T(8,128)S(1)}, ...), condition=%wide.region_4.5_spmd, body=%wide.region_3.4_spmd.sunk | while | flops 176357376 | bytes 2231425 | solution.py:162
  128.6 1.2 convolution_subtract_fusion.2
  131.0 1.8 fusion.127
  133.5 1.3 convolution_add_fusion.4
  137.1 1.8 fusion.127
  139.6 1.3 convolution_add_fusion.4
  143.2 1.8 fusion.127
  145.7 1.3 convolution_add_fusion.4
  149.3 1.8 fusion.127
  151.8 1.3 convolution_add_fusion.4
  155.4 1.8 fusion.127
  157.9 1.3 convolution_add_fusion.4
  161.5 1.8 fusion.127
  164.0 1.3 convolution_add_fusion.4
  165.2 1.2 convolution_subtract_fusion.2
  167.6 1.8 fusion.127
  170.1 1.3 convolution_add_fusion.4
  171.4 1.3 convolution_subtract_fusion.2
  173.8 1.8 fusion.127
  176.3 1.3 convolution_add_fusion.4
  177.6 11.2 %all-gather = f32[8,128,128]{2,1,0:T(8,128)} all-gather(f32[2,128,128]{2,1,0:T(8,128)S(1)} %get-tuple-element.243), channel_id=2, replica_groups=mesh['ep'=4,'tp'=8] {'ep'}, dimensions={0}, use_global_device_ids=true | all-gather | bytes 655360 | tf_op jit(solution)/shard_map/all_gather | solution.py:18
  188.8 11.2 %all-gather.1 = f32[8,128,128]{2,1,0:T(8,128)} all-gather(f32[2,128,128]{2,1,0:T(8,128)S(1)} %get-tuple-element.242), channel_id=3, replica_groups=mesh['ep'=4,'tp'=8] {'ep'}, dimensions={0}, use_global_device_ids=true | all-gather | bytes 655360 | tf_op jit(solution)/shard_map/all_gather | solution.py:18
  200.1 4.0 while.27
  200.1 1.2 fusion.130
  201.4 1.2 fusion.130
  202.7 1.2 fusion.130
  204.1 1.8 fusion.55
  206.2 2.1 convolution_convert_fusion
  208.4 12.9 %fusion.26 = f32[4,4,32,1024]{3,2,1,0:T(8,128)} fusion(bf16[4,1024,2048]{2,1,0:T(8,128)(2,1)} %all-gather.8.cloned.1.call-done, bf16[4,4,32,2048]{3,2,1,0:T(8,128)(2,1)S(1)} %all-to-all-done), kind=kOutput, calls=%fused_computation.34 | convolution fusion | flops 2147483648 | bytes 20971520 | tf_op jit(solution)/shard_map/secd,efd->secf/dot_general | solution.py:207
  221.3 93.1 %all-gather.6.cloned.1.call-done = bf16[4,1024,2048]{2,1,0:T(8,128)(2,1)} async-done(((bf16[4,128,2048]{2,1,0:T(8,128)(2,1)}), bf16[4,1024,2048]{2,1,0:T(8,128)(2,1)}) %all-gather.6.cloned.1.call-update) | async-done | bytes 16777232 | tf_op jit(solution)/shard_map/all_gather | solution.py:203
  314.3 13.1 %fusion.36 = bf16[4,4,32,1024]{3,2,0,1:T(8,128)(2,1)} fusion(f32[4,4,32,1024]{3,2,1,0:T(8,128)} %fusion.26, bf16[4,1024,2048]{2,1,0:T(8,128)(2,1)} %all-gather.6.cloned.1.call-done, bf16[4,4,32,2048]{3,2,1,0:T(8,128)(2,1)S(1)} %all-to-all-done), kind=kOutput, calls=%fused_computation.42 | convolution fusion | flops 2150629376 | bytes 22020096 | tf_op jit(solution)/shard_map/secd,efd->secf/dot_general | solution.py:206
  327.4 137.8 %all-gather.10.cloned.1.call-done = bf16[4,1024,2048]{2,1,0:T(8,128)(2,1)} async-done(((bf16[4,128,2048]{2,1,0:T(8,128)(2,1)}), bf16[4,1024,2048]{2,1,0:T(8,128)(2,1)}) %all-gather.10.cloned.1.call-update) | async-done | bytes 16777232 | tf_op jit(solution)/shard_map/all_gather | solution.py:205
  465.3 8.5 %fusion.33 = bf16[4,4,32,2048]{3,2,0,1:T(8,128)(2,1)S(1)} fusion(bf16[4,4,32,1024]{3,2,0,1:T(8,128)(2,1)} %fusion.36, bf16[4,1024,2048]{2,1,0:T(8,128)(2,1)} %all-gather.10.cloned.1.call-done), kind=kOutput, calls=%fused_computation.40 | convolution fusion | flops 2148532224 | bytes 19922944 | tf_op jit(solution)/shard_map/secf,efd->secd/dot_general | solution.py:209
  473.7 1.6 copy.119
  475.3 4.0 all-to-all-start.1
  479.9 24.7 %all-to-all-done.1 = bf16[4,4,32,2048]{3,2,1,0:T(8,128)(2,1)S(1)} async-done(((bf16[4,4,32,2048]{3,2,1,0:T(8,128)(2,1)}), bf16[4,4,32,2048]{3,2,1,0:T(8,128)(2,1)S(1)}, u32[]{:S(2)}, u32[]{:S(2)}) %all-to-all-start.1) | async-done | bytes 2097184 | tf_op jit(solution)/shard_map/all_to_all | solution.py:210
  504.6 2.3 gather_fusion.1
  507.0 1.7 gather.15
  508.7 4.9 multiply_reduce_fusion
  (148 shorter events, 39.8 us)
Async XLA Ops:
  7.2 199.1 %copy-start = (bf16[256,2048]{1,0:T(8,128)(2,1)S(1)}, bf16[256,2048]{1,0:T(8,128)(2,1)}, u32[]{:S(2)}) copy-start(bf16[256,2048]{1,0:T(8,128)(2,1)} %param.27) | copy-start | bytes 3145732
  7.2 201.2 %all-gather.8.cloned.1.call-start = ((), (), s32[]{:S(2)}) async-start(), calls=%async_computation.5 | async-start | bytes 18874368 | tf_op jit(solution)/shard_map/all_gather | solution.py:204
  7.9 1.5 copy-start.11
  7.9 5.2 %copy-start.2 = (bf16[128,2048]{1,0:T(8,128)(2,1)S(1)}, bf16[128,2048]{1,0:T(8,128)(2,1)}, u32[]{:S(2)}) copy-start(bf16[128,2048]{1,0:T(8,128)(2,1)} %param.28) | copy-start | bytes 1572868
  7.9 5.4 %copy-start.14 = (f32[2048]{0:T(1024)S(1)}, f32[2048]{0:T(1024)}, u32[]{:S(2)}) copy-start(f32[2048]{0:T(1024)} %param.29) | copy-start | bytes 24580
  7.9 306.4 %all-gather.6.cloned.1.call-start = ((), (), s32[]{:S(2)}) async-start(), calls=%async_computation.4 | async-start | bytes 18874368 | tf_op jit(solution)/shard_map/all_gather | solution.py:203
  8.7 456.6 %all-gather.10.cloned.1.call-start = ((), (), s32[]{:S(2)}) async-start(), calls=%async_computation.6 | async-start | bytes 18874368 | tf_op jit(solution)/shard_map/all_gather | solution.py:205
  11.0 0.6 copy-start.9
  11.6 1.5 copy-start.17
  20.0 5.6 %copy-start.23 = (f32[2]{0:T(128)S(1)}, f32[2]{0:T(128)}, u32[]{:S(2)}) copy-start(f32[2]{0:T(128)} %param.25) | copy-start | bytes 28
  20.0 5.6 %copy-start.19 = (f32[2,512]{1,0:T(2,128)S(1)}, f32[2,512]{1,0:T(2,128)}, u32[]{:S(2)}) copy-start(f32[2,512]{1,0:T(2,128)} %param.26) | copy-start | bytes 12292
  20.0 5.6 %copy-start.20 = (bf16[2,512]{1,0:T(2,128)(2,1)S(1)}, bf16[2,512]{1,0:T(2,128)(2,1)}, u32[]{:S(2)}) copy-start(bf16[2,512]{1,0:T(2,128)(2,1)} %param.24) | copy-start | bytes 6148
  20.0 5.8 %copy-start.6 = (bf16[512,256]{1,0:T(8,128)(2,1)S(1)}, bf16[512,256]{1,0:T(8,128)(2,1)}, u32[]{:S(2)}) copy-start(bf16[512,256]{1,0:T(8,128)(2,1)} %param.21) | copy-start | bytes 786436
  20.0 188.4 %all-to-all-start = ((bf16[4,4,32,2048]{3,2,1,0:T(8,128)(2,1)}), bf16[4,4,32,2048]{3,2,1,0:T(8,128)(2,1)S(1)}, u32[]{:S(2)}, u32[]{:S(2)}) async-start(bf16[4,4,32,2048]{3,2,1,0:T(8,128)(2,1)} %broadcast_select_fusion), calls=%async_computation.1 | async-start | bytes 4194304 | tf_op jit(solution)/shard_map/all_to_all | solution.py:202
  25.6 488.0 %reduce-scatter.2.cloned.1.call-start = ((), (), s32[]{:S(2)}) async-start(), calls=%async_computation.3 | async-start | bytes 2359296 | tf_op jit(solution)/shard_map/reduce_scatter | solution.py:178
  28.6 0.6 copy-start.15
  28.7 0.8 copy-start.4
  116.8 0.6 copy-start.13
  118.1 4.3 copy-start.7
  122.4 2.0 copy-start.3
  122.4 3.1 copy-start.5
  122.4 3.1 copy-start.8
  122.4 3.1 copy-start.16
  123.6 4.0 copy-start.21
  475.3 4.0 copy-start.10
  475.3 4.2 copy-start.12
  475.3 4.4 copy-start.24
  475.3 4.4 copy-start.22
  475.3 4.6 copy-start.18
  475.3 29.3 %all-to-all-start.1 = ((bf16[4,4,32,2048]{3,2,1,0:T(8,128)(2,1)}), bf16[4,4,32,2048]{3,2,1,0:T(8,128)(2,1)S(1)}, u32[]{:S(2)}, u32[]{:S(2)}) async-start(bf16[4,4,32,2048]{3,2,1,0:T(8,128)(2,1)} %copy.119), calls=%async_computation.2 | async-start | bytes 4194304 | tf_op jit(solution)/shard_map/all_to_all | solution.py:210
  504.6 9.0 %copy-start.1 = (bf16[256,2048]{1,0:T(8,128)(2,1)S(1)}, bf16[256,2048]{1,0:T(8,128)(2,1)}, u32[]{:S(2)}) copy-start(bf16[256,2048]{1,0:T(8,128)(2,1)} %param.27) | copy-start | bytes 3145732
Sparse Core Ops, SparseCore 0:
  9.6 153.7 all-gather.7
  165.0 149.2 all-gather.5
  316.0 149.2 all-gather.9
  468.0 34.1 reduce-scatter.1
where the time goes:
time: 522 us; the launch traced here: 520 us
  waiting for transfers between devices  258 us (49%)
  other arithmetic  98.3 us (19%)
  matrix products  91.2 us (17%)
  local copies, waits for them, and re-layouts  26 us (5%)
  blocking collectives  22.5 us (4%)
  between operations  14.2 us (3%)
  starting transfers between devices  9.7 us (2%)
    all_gather x1, waiting for transfers between devices, shards(): down_piece = lax.all_gather(expert_down_weight, 'tp', axis=1, tiled=True)  138 us
    all_gather x1, waiting for transfers between devices, shards(): gate_piece = lax.all_gather(expert_gate_weight, 'tp', axis=1, tiled=True)  93.1 us
    another operation x2, other arithmetic, block_terms(): jax.scipy.linalg.solve_triangular(system, rhs_cols, lower=True, unit_diag...  80 us
    all_to_all x1, waiting for transfers between devices, shards(): lax.all_to_all(produced.astype(jnp.bfloat16), 'ep', split_axis=0, concat_...  24.7 us
    all_gather x2, blocking collectives, prefix(): pieces = jax.tree.map(lambda part: lax.all_gather(part, axis), value)  22.5 us
    dot_general x8, matrix products, carry_step(): jnp.einsum('hcj,hjv->hcv', scores, value_updates, precision=precise_setting)  14.2 us
    dot_general x1, matrix products, shards(): jnp.einsum('secd,efd->secf', arrived, gate_piece, preferred_element_type=...  13.1 us
    dot_general x1, matrix products, shards(): jnp.einsum('secd,efd->secf', arrived, up_piece, preferred_element_type=jn...  12.9 us
  transfers between devices with their start and end apart: 6, of which 3 were waited for; matrix products, arithmetic and copies ran while one was open for 41% of the time, Pallas kernels for 0%

commit v1 on v0

--- a/solution.py
+++ b/solution.py
@@ -11,6 +11,18 @@
 TOPK = 2
 precise_setting = lax.Precision.HIGHEST
 norm_eps = 1e-06
+
+
+def ring_product(value, axis, dim, contribution):
+    size, index = (lax.axis_size(axis), lax.axis_index(axis))
+    left = [(i, (i - 1) % size) for i in range(size)]
+    extent = value.shape[dim]
+    carried = value
+    running = contribution(carried, index * extent)
+    for step in range(1, size):
+        carried = lax.ppermute(carried, axis, left)
+        running = running + contribution(carried, (index + step) % size * extent)
+    return running
 
 
 def prefix(value, axis, join, neutral):
@@ -202,11 +214,20 @@
     arrived = lax.all_to_all(outgoing, "ep", split_axis=0, concat_axis=0, tiled=True)
     gate_piece = lax.all_gather(expert_gate_weight, "tp", axis=1, tiled=True)
     up_piece = lax.all_gather(expert_up_weight, "tp", axis=1, tiled=True)
-    down_piece = lax.all_gather(expert_down_weight, "tp", axis=1, tiled=True)
     gating = jnp.einsum("secd,efd->secf", arrived, gate_piece, preferred_element_type=jnp.float32)
     upward = jnp.einsum("secd,efd->secf", arrived, up_piece, preferred_element_type=jnp.float32)
     hidden = (jax.nn.silu(gating) * upward).astype(jnp.bfloat16)
-    produced = jnp.einsum("secf,efd->secd", hidden, down_piece, preferred_element_type=jnp.float32)
+    produced = ring_product(
+        expert_down_weight,
+        "tp",
+        1,
+        lambda own_block, at: jnp.einsum(
+            "secf,efd->secd",
+            lax.dynamic_slice_in_dim(hidden, at, own_block.shape[1], axis=3),
+            own_block,
+            preferred_element_type=jnp.float32,
+        ),
+    )
     returned = lax.all_to_all(
         produced.astype(jnp.bfloat16), "ep", split_axis=0, concat_axis=0, tiled=True
     )

time: 522 us -> 542 us (1.038)
  the two profiles are of different devices: /device:TPU:0 before, /device:TPU:24 now
where the time goes in v1:
time: 542 us; the launch traced here: 540 us
  waiting for transfers between devices  250 us (46%)
  matrix products  112 us (21%)
  other arithmetic  100 us (18%)
  starting transfers between devices  22.3 us (4%)
  blocking collectives  22 us (4%)
  local copies, waits for them, and re-layouts  18.5 us (3%)
  between operations  14.3 us (3%)
    ppermute x7, waiting for transfers between devices, ring_product(): carried = lax.ppermute(carried, axis, left)  197 us
    another operation x2, other arithmetic, block_terms(): jax.scipy.linalg.solve_triangular(system, rhs_cols, lower=True, unit_diag...  80 us
    dot_general x8, matrix products, shards(): jnp.einsum('secf,efd->secd', lax.dynamic_slice_in_dim(hidden, at, own_blo...  31.6 us
    all_gather x1, waiting for transfers between devices, shards(): gate_piece = lax.all_gather(expert_gate_weight, 'tp', axis=1, tiled=True)  26.9 us
    all_to_all x1, waiting for transfers between devices, shards(): lax.all_to_all(produced.astype(jnp.bfloat16), 'ep', split_axis=0, concat_...  25 us
    all_gather x2, blocking collectives, prefix(): pieces = jax.tree.map(lambda part: lax.all_gather(part, axis), value)  22 us
    ppermute x7, starting transfers between devices, ring_product(): carried = lax.ppermute(carried, axis, left)  14.5 us
    dot_general x8, matrix products, carry_step(): jnp.einsum('hcj,hjv->hcv', scores, value_updates, precision=precise_setting)  14.1 us
  transfers between devices with their start and end apart: 12, of which 6 were waited for; matrix products, arithmetic and copies ran while one was open for 43% of the time, Pallas kernels for 0%

profile of v1, /device:TPU:24, one launch (start us, length us, event | category | flops | bytes accessed | tf_op | source)
XLA Modules:
  0.0 539.6 jit_solution(5116004035360359934)
XLA Ops:
  8.9 46.6 %collective-permute-done = bf16[4,128,2048]{2,1,0:T(8,128)(2,1)} collective-permute-done((bf16[4,128,2048]{2,1,0:T(8,128)(2,1)S(1)}, bf16[4,128,2048]{2,1,0:T(8,128)(2,1)}, u32[]{:S(2)}, u32[]{:S(2)}) %collective-permute-start) | collective-permute-done | bytes 2097184 | tf_op jit(solution)/shard_map/ppermute | solution.py:23
  55.5 2.3 collective-permute-start.1
  60.8 65.9 %collective-permute-done.1 = bf16[4,128,2048]{2,1,0:T(8,128)(2,1)} collective-permute-done((bf16[4,128,2048]{2,1,0:T(8,128)(2,1)}, bf16[4,128,2048]{2,1,0:T(8,128)(2,1)}, u32[]{:S(2)}, u32[]{:S(2)}) %collective-permute-start.1) | collective-permute-done | bytes 2097184 | tf_op jit(solution)/shard_map/ppermute | solution.py:23
  126.7 2.2 collective-permute-start.2
  131.5 3.3 gather_fusion
  134.8 3.1 broadcast_select_fusion
  138.0 4.0 all-to-all-start
  142.3 55.6 %collective-permute-done.2 = bf16[4,128,2048]{2,1,0:T(8,128)(2,1)} collective-permute-done((bf16[4,128,2048]{2,1,0:T(8,128)(2,1)}, bf16[4,128,2048]{2,1,0:T(8,128)(2,1)}, u32[]{:S(2)}, u32[]{:S(2)}) %collective-permute-start.2) | collective-permute-done | bytes 2097184 | tf_op jit(solution)/shard_map/ppermute | solution.py:23
  197.9 2.2 collective-permute-start.3
  203.2 2.2 fusion.60
  206.3 28.4 %collective-permute-done.3 = bf16[4,128,2048]{2,1,0:T(8,128)(2,1)} collective-permute-done((bf16[4,128,2048]{2,1,0:T(8,128)(2,1)}, bf16[4,128,2048]{2,1,0:T(8,128)(2,1)}, u32[]{:S(2)}, u32[]{:S(2)}) %collective-permute-start.3) | collective-permute-done | bytes 2097184 | tf_op jit(solution)/shard_map/ppermute | solution.py:23
  234.8 1.9 collective-permute-start.4
  236.7 80.0 %custom-call.4 = f32[2,8,1,64,64]{3,4,2,1,0:T(8,128)} custom-call(f32[2,8,1,64,64]{4,3,2,1,0:T(8,128)} %fusion.60), custom_call_target="InvertDiagBlocksLowerTriangular" | custom-call | tf_op jit(solution)/shard_map/jit(_solve_triangular)/vmap(vmap())/triangular_solve | solution.py:64
  316.7 2.0 copy.100
  320.1 2.5 multiply_multiply_fusion
  325.7 2.0 fusion.58
  328.8 5.6 %collective-permute-start.5 = (bf16[4,128,2048]{2,1,0:T(8,128)(2,1)}, bf16[4,128,2048]{2,1,0:T(8,128)(2,1)}, u32[]{:S(2)}, u32[]{:S(2)}) collective-permute-start(bf16[4,128,2048]{2,1,0:T(8,128)(2,1)} %collective-permute-done.4), channel_id=1, source_target_pairs={{0,7},{1,0},{2,1},{3,2},{4,3},{5,4},{6,5},{7,6},{8,15},{9,8},{10,9... | collective-permute-start | bytes 6291464 | tf_op jit(solution)/shard_map/ppermute | solution.py:23
  334.4 43.4 %while.26 = (s32[]{:T(128)}, f32[2,128,256]{2,1,0:T(8,128)S(1)}, f32[8,2,64,256]{3,2,0,1:T(8,128)}, f32[8,2]{1,0:T(8,128)S(1)}, f32[8,2,64,128]{3,2,0,1:T(8,128)...) while((s32[]{:T(128)}, f32[2,128,256]{2,1,0:T(8,128)S(1)}, ...), condition=%wide.region_4.5_spmd, body=%wide.region_3.4_spmd.sunk | while | flops 176357376 | bytes 2231425 | solution.py:174
  336.9 1.8 fusion.150
  342.3 1.8 fusion.150
  347.7 1.8 fusion.150
  353.1 1.8 fusion.150
  358.5 1.8 fusion.150
  363.9 1.8 fusion.150
  369.4 1.8 fusion.150
  374.8 1.8 fusion.150
  377.9 11.5 %all-gather = f32[8,128,128]{2,1,0:T(8,128)} all-gather(f32[2,128,128]{2,1,0:T(8,128)S(1)} %get-tuple-element.243), channel_id=2, replica_groups=mesh['ep'=4,'tp'=8] {'ep'}, dimensions={0}, use_global_device_ids=true | all-gather | bytes 655360 | tf_op jit(solution)/shard_map/all_gather | solution.py:30
  389.4 10.5 %all-gather.1 = f32[8,128,128]{2,1,0:T(8,128)} all-gather(f32[2,128,128]{2,1,0:T(8,128)S(1)} %get-tuple-element.242), channel_id=3, replica_groups=mesh['ep'=4,'tp'=8] {'ep'}, dimensions={0}, use_global_device_ids=true | all-gather | bytes 655360 | tf_op jit(solution)/shard_map/all_gather | solution.py:30
  399.9 3.8 while.27
  403.7 1.8 fusion.63
  405.8 2.0 convolution_convert_fusion
  408.2 12.7 %fusion.24 = f32[4,4,32,1024]{3,2,1,0:T(8,128)} fusion(bf16[4,1024,2048]{2,1,0:T(8,128)(2,1)} %all-gather.7.cloned.1.call-done, bf16[4,4,32,2048]{3,2,1,0:T(8,128)(2,1)S(1)} %all-to-all-done), kind=kOutput, calls=%fused_computation.32 | convolution fusion | flops 2147483648 | bytes 20971520 | tf_op jit(solution)/shard_map/secd,efd->secf/dot_general | solution.py:218
  421.0 26.9 %all-gather.5.cloned.1.call-done = bf16[4,1024,2048]{2,1,0:T(8,128)(2,1)} async-done(((bf16[4,128,2048]{2,1,0:T(8,128)(2,1)}), bf16[4,1024,2048]{2,1,0:T(8,128)(2,1)}) %all-gather.5.cloned.1.call-update) | async-done | bytes 16777232 | tf_op jit(solution)/shard_map/all_gather | solution.py:215
  447.9 12.1 %fusion.44 = bf16[4,4,32,1024]{3,2,0,1:T(8,128)(2,1)S(1)} fusion(f32[4,4,32,1024]{3,2,1,0:T(8,128)} %fusion.24, bf16[4,1024,2048]{2,1,0:T(8,128)(2,1)} %all-gather.5.cloned.1.call-done, bf16[4,4,32,2048]{3,2,1,0:T(8,128)(2,1)S(1)} %all-to-all-done), kind=kOutput, calls=%fused_computation.55 | convolution fusion | flops 2150629376 | bytes 22020096 | tf_op jit(solution)/shard_map/secd,efd->secf/dot_general | solution.py:217
  460.0 2.3 fusion.42
  462.3 2.3 fusion.30
  464.7 2.3 fusion.32
  467.0 2.3 fusion.34
  469.3 4.3 fusion.36
  473.6 4.3 fusion.38
  477.8 4.5 fusion.40
  482.4 9.2 %fusion.28 = bf16[4,4,32,2048]{3,2,0,1:T(8,128)(2,1)} fusion(f32[4,4,32,2048]{3,2,1,0:T(8,128)S(1)} %fusion.30, f32[4,4,32,2048]{3,2,1,0:T(8,128)S(1)} %fusion.32, f32[4,4,32,2048]{3,2,1,0:T(8,128)S(1)} %fusion.34, f32[4,4,32,2048]{3,2,1,0:T(8,128)} %fusion.36, f32[4,4,32,2048]{3,2,1,0:T(8,128)} %fusion.38, f32[4,4,32,2048]{3,2,1,0:T(8,128)S(1)} %fusion.42, ...), kind=kOutput, calls=%fused_computation.38 | convolution fusion | flops 276824064 | bytes 33685508 | tf_op jit(solution)/shard_map/secf,efd->secd/dot_general | solution.py:224
  491.6 3.2 copy.119
  494.8 3.7 all-to-all-start.1
  499.0 25.0 %all-to-all-done.1 = bf16[4,4,32,2048]{3,2,1,0:T(8,128)(2,1)S(1)} async-done(((bf16[4,4,32,2048]{3,2,1,0:T(8,128)(2,1)}), bf16[4,4,32,2048]{3,2,1,0:T(8,128)(2,1)S(1)}, u32[]{:S(2)}, u32[]{:S(2)}) %all-to-all-start.1) | async-done | bytes 2097184 | tf_op jit(solution)/shard_map/all_to_all | solution.py:231
  524.0 2.3 gather_fusion.1
  526.4 1.7 gather.15
  528.1 4.9 multiply_reduce_fusion
  (150 shorter events, 50.9 us)
Async XLA Ops:
  7.2 398.6 %copy-start = (bf16[256,2048]{1,0:T(8,128)(2,1)S(1)}, bf16[256,2048]{1,0:T(8,128)(2,1)}, u32[]{:S(2)}) copy-start(bf16[256,2048]{1,0:T(8,128)(2,1)} %param.27) | copy-start | bytes 3145732
  7.2 1.7 copy-start.2
  7.2 50.6 %copy-start.8 = (s32[128,2]{0,1:T(2,128)S(1)}, s32[128,2]{0,1:T(2,128)}, u32[]{:S(2)}) copy-start(s32[128,2]{0,1:T(2,128)} %param.30) | copy-start | bytes 3076
  7.2 123.1 %copy-start.9 = (f32[2048]{0:T(1024)S(1)}, f32[2048]{0:T(1024)}, u32[]{:S(2)}) copy-start(f32[2048]{0:T(1024)} %param.29) | copy-start | bytes 24580
  7.2 401.0 %all-gather.7.cloned.1.call-start = ((), (), s32[]{:S(2)}) async-start(), calls=%async_computation.5 | async-start | bytes 18874368 | tf_op jit(solution)/shard_map/all_gather | solution.py:216
  7.9 440.0 %all-gather.5.cloned.1.call-start = ((), (), s32[]{:S(2)}) async-start(), calls=%async_computation.4 | async-start | bytes 18874368 | tf_op jit(solution)/shard_map/all_gather | solution.py:215
  8.9 46.6 %collective-permute-start = (bf16[4,128,2048]{2,1,0:T(8,128)(2,1)S(1)}, bf16[4,128,2048]{2,1,0:T(8,128)(2,1)}, u32[]{:S(2)}, u32[]{:S(2)}) collective-permute-start(bf16[4,128,2048]{2,1,0:T(8,128)(2,1)S(1)} %copy-done.2), channel_id=1, source_target_pairs={{0,7},{1,0},{2,1},{3,2},{4,3},{5,4},{6,5},{7,6},{8,15},{9,8},{10,9... | collective-permute-start | bytes 6291464 | tf_op jit(solution)/shard_map/ppermute | solution.py:23
  55.5 71.2 %collective-permute-start.1 = (bf16[4,128,2048]{2,1,0:T(8,128)(2,1)}, bf16[4,128,2048]{2,1,0:T(8,128)(2,1)}, u32[]{:S(2)}, u32[]{:S(2)}) collective-permute-start(bf16[4,128,2048]{2,1,0:T(8,128)(2,1)} %collective-permute-done), channel_id=1, source_target_pairs={{0,7},{1,0},{2,1},{3,2},{4,3},{5,4},{6,5},{7,6},{8,15},{9,8},{10,9... | collective-permute-start | bytes 6291464 | tf_op jit(solution)/shard_map/ppermute | solution.py:23
  126.7 71.1 %collective-permute-start.2 = (bf16[4,128,2048]{2,1,0:T(8,128)(2,1)}, bf16[4,128,2048]{2,1,0:T(8,128)(2,1)}, u32[]{:S(2)}, u32[]{:S(2)}) collective-permute-start(bf16[4,128,2048]{2,1,0:T(8,128)(2,1)} %collective-permute-done.1), channel_id=1, source_target_pairs={{0,7},{1,0},{2,1},{3,2},{4,3},{5,4},{6,5},{7,6},{8,15},{9,8},{10,9... | collective-permute-start | bytes 6291464 | tf_op jit(solution)/shard_map/ppermute | solution.py:23
  137.9 4.0 copy-start.6
  137.9 4.2 copy-start.15
  138.0 4.3 copy-start.10
  138.0 4.3 copy-start.12
  138.0 62.3 %copy-start.11 = (bf16[2,512]{1,0:T(2,128)(2,1)S(1)}, bf16[2,512]{1,0:T(2,128)(2,1)}, u32[]{:S(2)}) copy-start(bf16[2,512]{1,0:T(2,128)(2,1)} %param.23) | copy-start | bytes 6148
  138.0 270.2 %all-to-all-start = ((bf16[4,4,32,2048]{3,2,1,0:T(8,128)(2,1)}), bf16[4,4,32,2048]{3,2,1,0:T(8,128)(2,1)S(1)}, u32[]{:S(2)}, u32[]{:S(2)}) async-start(bf16[4,4,32,2048]{3,2,1,0:T(8,128)(2,1)} %broadcast_select_fusion), calls=%async_computation.1 | async-start | bytes 4194304 | tf_op jit(solution)/shard_map/all_to_all | solution.py:214
  142.0 391.0 %reduce-scatter.2.cloned.1.call-start = ((), (), s32[]{:S(2)}) async-start(), calls=%async_computation.3 | async-start | bytes 2359296 | tf_op jit(solution)/shard_map/reduce_scatter | solution.py:190
  197.9 36.9 %collective-permute-start.3 = (bf16[4,128,2048]{2,1,0:T(8,128)(2,1)}, bf16[4,128,2048]{2,1,0:T(8,128)(2,1)}, u32[]{:S(2)}, u32[]{:S(2)}) collective-permute-start(bf16[4,128,2048]{2,1,0:T(8,128)(2,1)} %collective-permute-done.2), channel_id=1, source_target_pairs={{0,7},{1,0},{2,1},{3,2},{4,3},{5,4},{6,5},{7,6},{8,15},{9,8},{10,9... | collective-permute-start | bytes 6291464 | tf_op jit(solution)/shard_map/ppermute | solution.py:23
  203.2 3.1 copy-start.4
  234.8 94.0 %collective-permute-start.4 = (bf16[4,128,2048]{2,1,0:T(8,128)(2,1)}, bf16[4,128,2048]{2,1,0:T(8,128)(2,1)}, u32[]{:S(2)}, u32[]{:S(2)}) collective-permute-start(bf16[4,128,2048]{2,1,0:T(8,128)(2,1)} %collective-permute-done.3), channel_id=1, source_target_pairs={{0,7},{1,0},{2,1},{3,2},{4,3},{5,4},{6,5},{7,6},{8,15},{9,8},{10,9... | collective-permute-start | bytes 6291464 | tf_op jit(solution)/shard_map/ppermute | solution.py:23
  318.9 3.6 copy-start.7
  322.5 2.0 copy-start.3
  322.5 3.2 copy-start.5
  323.6 4.0 copy-start.13
  328.8 79.2 %collective-permute-start.5 = (bf16[4,128,2048]{2,1,0:T(8,128)(2,1)}, bf16[4,128,2048]{2,1,0:T(8,128)(2,1)}, u32[]{:S(2)}, u32[]{:S(2)}) collective-permute-start(bf16[4,128,2048]{2,1,0:T(8,128)(2,1)} %collective-permute-done.4), channel_id=1, source_target_pairs={{0,7},{1,0},{2,1},{3,2},{4,3},{5,4},{6,5},{7,6},{8,15},{9,8},{10,9... | collective-permute-start | bytes 6291464 | tf_op jit(solution)/shard_map/ppermute | solution.py:23
  408.0 74.4 %collective-permute-start.6 = (bf16[4,128,2048]{2,1,0:T(8,128)(2,1)}, bf16[4,128,2048]{2,1,0:T(8,128)(2,1)}, u32[]{:S(2)}, u32[]{:S(2)}) collective-permute-start(bf16[4,128,2048]{2,1,0:T(8,128)(2,1)} %collective-permute-done.5), channel_id=1, source_target_pairs={{0,7},{1,0},{2,1},{3,2},{4,3},{5,4},{6,5},{7,6},{8,15},{9,8},{10,9... | collective-permute-start | bytes 6291464 | tf_op jit(solution)/shard_map/ppermute | solution.py:23
  494.8 4.1 copy-start.16
  494.8 4.1 copy-start.14
  494.8 29.3 %all-to-all-start.1 = ((bf16[4,4,32,2048]{3,2,1,0:T(8,128)(2,1)}), bf16[4,4,32,2048]{3,2,1,0:T(8,128)(2,1)S(1)}, u32[]{:S(2)}, u32[]{:S(2)}) async-start(bf16[4,4,32,2048]{3,2,1,0:T(8,128)(2,1)} %copy.119), calls=%async_computation.2 | async-start | bytes 4194304 | tf_op jit(solution)/shard_map/all_to_all | solution.py:231
  524.0 9.0 %copy-start.1 = (bf16[256,2048]{1,0:T(8,128)(2,1)S(1)}, bf16[256,2048]{1,0:T(8,128)(2,1)}, u32[]{:S(2)}) copy-start(bf16[256,2048]{1,0:T(8,128)(2,1)} %param.27) | copy-start | bytes 3145732
Sparse Core Ops, SparseCore 0:
  9.6 231.0 all-gather.6
  242.3 205.5 all-gather.4
  450.8 31.3 reduce-scatter.1
